TPU v7x, 32 devices: a whole 2x2x4 slice. The times are simulated.
32 devices in a mesh: grp: 1, ep: 32 (over z, y, x, core).
Axes of the slice: x: 2, y: 2, z: 4, core: 2. Of those that a mesh axis runs over, the one named last changes fastest.
Arguments:
- tokens: bfloat16 [64, 2048], P('grp', 'ep'), may hold values from -6 to 6
- w_query: bfloat16 [2048, 1024], P('ep'), may hold values from -0.125 to 0.125
- w_key: bfloat16 [2048, 1024], P('ep'), may hold values from -0.125 to 0.125
- w_value: bfloat16 [2048, 1024], P('ep'), may hold values from -0.125 to 0.125
- w_forget: bfloat16 [2048, 16], P('ep'), may hold values from -0.125 to 0.125
- forget_bias: float32 [16], replicated, may hold values from -1 to 2
- cache_keys: bfloat16 [64, 1024, 1024], P(('grp', 'ep'))
- cache_values: bfloat16 [64, 1024, 1024], P(('grp', 'ep')), may hold values from -6 to 6
- cache_gates: float32 [64, 1024, 16], P(('grp', 'ep')), as said below
- lengths: int32 [64], P(('grp', 'ep')), may hold values from 128 to 1024, as said below
- w_out: bfloat16 [1024, 2048], P('ep'), may hold values from -0.1875 to 0.1875
- norm_gain: bfloat16 [2048], replicated, may hold values from 0.099609375 to 1.8984375
- w_router: bfloat16 [2048, 4], replicated, may hold values from -0.125 to 0.125
- routes: int32 [64, 2], P('grp'), may hold values from 0 to 3, all different within a row
- dense_gate: bfloat16 [2048], replicated, may hold values from -0.25 to 0.25
- dense_w_gate: bfloat16 [2048, 8192], P(None, 'ep'), may hold values from -0.125 to 0.125
- dense_w_up: bfloat16 [2048, 8192], P(None, 'ep'), may hold values from -0.125 to 0.125
- dense_w_down: bfloat16 [8192, 2048], P('ep'), may hold values from -0.125 to 0.125
- expert_w_gate: bfloat16 [2048, 16384], P(None, 'ep'), may hold values from -0.125 to 0.125
- expert_w_up: bfloat16 [2048, 16384], P(None, 'ep'), may hold values from -0.125 to 0.125
- expert_w_down: bfloat16 [16384, 2048], P('ep'), may hold values from -0.1875 to 0.1875
- final_gain: bfloat16 [2048], P('ep'), may hold values from 0.099609375 to 1.8984375
Outputs:
- result: bfloat16 [64, 2048], P('grp', 'ep')
Inputs may be any that keep to these rules, and one draw needn't show every extreme that they name: `routes`: each row names 2 different experts; every expert is named by some row. `lengths`: the first sequence of each part holds 1024 positions. `cache_gates`: never rising along positions.
All inputs are finite; a program needn't handle non-finite values.
Results may differ from a plain program's by a relative error of at most 0.0085.
Values may be sent and summed in bfloat16 or wider, within the bound.
A program may use at most 128 MiB of HBM per device.

v0:
```python
import jax
import jax.numpy as jnp
from jax import lax
from jax.sharding import PartitionSpec as P

EXP_SPLIT = 8


norm_eps = 1e-05
residual_scale = 8.0**0.25


def norm_rows(values, weights):
    center = jnp.mean(values, axis=-1, keepdims=True)
    second = jnp.mean(values * values, axis=-1, keepdims=True)
    return (
        (values - center)
        * lax.rsqrt(second - center * center + norm_eps)
        * weights.astype(jnp.float32)
    )


def attend(
    query,
    new_key,
    new_value,
    forget_pre,
    forget_bias,
    cache_keys,
    cache_values,
    cache_gates,
    lengths,
):
    seqs_here, width = query.shape
    heads = cache_gates.shape[2]
    head_size = width // heads
    cache_len = cache_keys.shape[1]
    query = query.reshape(seqs_here, heads, head_size)
    new_key = new_key.reshape(seqs_here, heads, head_size)
    new_value = new_value.reshape(seqs_here, heads, head_size)
    keys_all = cache_keys.reshape(seqs_here, cache_len, heads, head_size)
    values_all = cache_values.reshape(seqs_here, cache_len, heads, head_size)
    log_gate = jax.nn.log_sigmoid(forget_pre + forget_bias[None, :])
    position = jnp.arange(cache_len, dtype=jnp.int32)
    is_last = (position[None, :] == (lengths - 1)[:, None]).astype(jnp.float32)
    last_gate = jnp.sum(cache_gates * is_last[:, :, None], axis=1)
    bias = (last_gate + log_gate)[:, :, None] - jnp.transpose(cache_gates, (0, 2, 1))
    scale = head_size ** (-0.5)
    scores = (
        jnp.einsum("shd,slhd->shl", query, keys_all, preferred_element_type=jnp.float32) * scale
        + bias
    )
    valid = (position[None, :] < lengths[:, None])[:, None, :]
    scores = jnp.where(valid, scores, -jnp.inf)
    own_score = jnp.sum(query.astype(jnp.float32) * new_key.astype(jnp.float32), axis=-1) * scale
    top = jnp.maximum(jnp.max(scores, axis=-1), own_score)
    weights_cache = jnp.exp(scores - top[:, :, None])
    weight_own = jnp.exp(own_score - top)
    total = jnp.sum(weights_cache, axis=-1) + weight_own
    probs = (weights_cache / total[:, :, None]).astype(jnp.bfloat16)
    prob_own = (weight_own / total).astype(jnp.bfloat16)
    mixed = jnp.einsum("shl,slhd->shd", probs, values_all, preferred_element_type=jnp.float32)
    mixed = mixed + prob_own.astype(jnp.float32)[:, :, None] * new_value.astype(jnp.float32)
    return mixed.astype(jnp.bfloat16).reshape(seqs_here, width)


def shards(
    tokens,
    w_query,
    w_key,
    w_value,
    w_forget,
    forget_bias,
    cache_keys,
    cache_values,
    cache_gates,
    lengths,
    w_out,
    norm_gain,
    w_router,
    routes,
    dense_gate,
    dense_w_gate,
    dense_w_up,
    dense_w_down,
    expert_w_gate,
    expert_w_up,
    expert_w_down,
    final_gain,
):
    rank = lax.axis_index("ep")
    seqs_all, feat_dev = tokens.shape
    offset = rank * feat_dev
    terms = (
        jnp.dot(tokens, w_query, preferred_element_type=jnp.float32),
        jnp.dot(tokens, w_key, preferred_element_type=jnp.float32),
        jnp.dot(tokens, w_value, preferred_element_type=jnp.float32),
        jnp.dot(tokens, w_forget, preferred_element_type=jnp.float32),
    )
    query_sum, key_sum, value_sum, forget_pre = (
        lax.psum_scatter(terms[0], "ep", scatter_dimension=0, tiled=True),
        lax.psum_scatter(terms[1], "ep", scatter_dimension=0, tiled=True),
        lax.psum_scatter(terms[2], "ep", scatter_dimension=0, tiled=True),
        lax.psum_scatter(terms[3], "ep", scatter_dimension=0, tiled=True),
    )
    attn = attend(
        query_sum.astype(jnp.bfloat16),
        key_sum.astype(jnp.bfloat16),
        value_sum.astype(jnp.bfloat16),
        forget_pre,
        forget_bias,
        cache_keys,
        cache_values,
        cache_gates,
        lengths,
    )
    head_cols = lax.all_to_all(attn, "ep", split_axis=1, concat_axis=0, tiled=True)
    partial_sum = jnp.dot(head_cols, w_out, preferred_element_type=jnp.float32)
    residual = residual_scale * tokens.astype(jnp.float32)
    placed = lax.dynamic_slice_in_dim(partial_sum, offset, feat_dev, 1) + residual
    mixed = lax.psum(lax.dynamic_update_slice_in_dim(partial_sum, placed, offset, 1), "ep")
    normed = norm_rows(mixed, norm_gain).astype(jnp.bfloat16)
    logits = jnp.dot(normed, w_router, preferred_element_type=jnp.float32)
    expert_count = w_router.shape[1]
    picks = (routes[:, :, None] == jnp.arange(expert_count, dtype=jnp.int32)[None, None, :]).astype(
        jnp.float32
    )
    chosen = jnp.sum(logits[:, None, :] * picks, axis=-1)
    route_weight = jax.nn.softmax(chosen, axis=-1)
    expert_id = rank // EXP_SPLIT
    mine = jnp.sum(route_weight * (routes == expert_id).astype(jnp.float32), axis=1)
    expert_gate_part = jnp.dot(normed, expert_w_gate, preferred_element_type=jnp.float32)
    expert_up_part = jnp.dot(normed, expert_w_up, preferred_element_type=jnp.float32)
    expert_hidden = (mine[:, None] * jax.nn.silu(expert_gate_part) * expert_up_part).astype(
        jnp.bfloat16
    )
    dense_scale = jax.nn.sigmoid(jnp.dot(normed, dense_gate, preferred_element_type=jnp.float32))
    dense_gate_part = jnp.dot(normed, dense_w_gate, preferred_element_type=jnp.float32)
    dense_up_part = jnp.dot(normed, dense_w_up, preferred_element_type=jnp.float32)
    dense_hidden = (dense_scale[:, None] * jax.nn.silu(dense_gate_part) * dense_up_part).astype(
        jnp.bfloat16
    )
    local_branch = jnp.dot(
        expert_hidden, expert_w_down, preferred_element_type=jnp.float32
    ) + jnp.dot(dense_hidden, dense_w_down, preferred_element_type=jnp.float32)
    branch = lax.psum(local_branch, "ep")
    final = residual_scale * normed.astype(jnp.float32) + branch
    center = jnp.mean(final, axis=-1, keepdims=True)
    second = jnp.mean(final * final, axis=-1, keepdims=True)
    unit = (final - center) * lax.rsqrt(second - center * center + norm_eps)
    result = (
        lax.dynamic_slice_in_dim(unit, offset, feat_dev, 1)
        * final_gain.astype(jnp.float32)[None, :]
    )
    return result.astype(jnp.bfloat16)


def solution(mesh):
    placed = (
        P("grp", "ep"),
        P("ep", None),
        P("ep", None),
        P("ep", None),
        P("ep", None),
        P(),
        P(("grp", "ep"), None, None),
        P(("grp", "ep"), None, None),
        P(("grp", "ep"), None, None),
        P(("grp", "ep")),
        P("ep", None),
        P(),
        P(),
        P("grp", None),
        P(),
        P(None, "ep"),
        P(None, "ep"),
        P("ep", None),
        P(None, "ep"),
        P(None, "ep"),
        P("ep", None),
        P("ep"),
    )
    return jax.shard_map(
        shards, mesh=mesh, in_specs=placed, out_specs=P("grp", "ep"), check_vma=False
    )
```

profile of v0, /device:TPU:0, one launch (start us, length us, event | category | flops | bytes accessed | tf_op | source)
XLA Modules:
  0.0 374.7 jit_solution(17475962631380918628)
XLA Ops:
  6.5 0.0 copy-start
  6.5 0.8 broadcast_add_fusion
  7.3 0.7 iota_compare_fusion
  8.1 0.8 fusion.49
  8.9 1.1 fusion.47
  10.0 1.1 fusion.50
  11.1 1.1 fusion.51
  12.2 52.3 %all-reduce.12 = (bf16[64,1024]{1,0:T(8,128)(2,1)S(1)}, f32[64,16]{1,0:T(8,128)S(1)}, bf16[64,1024]{1,0:T(8,128)(2,1)S(1)}, bf16[64,1024]{1,0:T(8,128)(2,1)S(1)}) all-reduce(f32[64,1024]{1,0:T(8,128)S(1)} %fusion.47, f32[64,16]{1,0:T(8,128)S(1)} %fusion.49, f32[64,1024]{1,0:T(8,128)S(1)} %fusion.50, ...), channel_id=2, replica_groups=mesh['grp'=1,'ep'=32] {'ep'}, use_global_device_ids=true, to_apply=%region_0.0.clone | all-reduce | flops 197632 | bytes 1187840
  64.5 0.1 reshape.129
  64.6 0.1 reshape.141
  64.7 0.1 compare_convert_fusion
  64.8 0.1 reshape.133
  64.9 0.1 reshape.132
  65.0 0.0 copy-start.3
  65.0 6.2 %copy.39 = bf16[2,1024,1024]{1,2,0:T(8,128)(2,1)} copy(bf16[2,1024,1024]{2,1,0:T(8,128)(2,1)} %param.28) | data formatting | bytes 8388608 | tf_op args[6]
  71.2 0.0 copy-done.3
  71.2 0.1 multiply_reduce_fusion.2
  71.3 0.1 multiply_reduce_fusion.3
  71.4 0.0 copy-start.10
  71.4 2.9 fusion.48
  74.3 0.0 copy-done.10
  74.3 0.2 fusion.45
  74.5 0.2 fusion.16
  74.7 0.1 fusion.25
  74.8 6.2 %copy.40 = bf16[2,1024,1024]{1,2,0:T(8,128)(2,1)} copy(bf16[2,1024,1024]{2,1,0:T(8,128)(2,1)} %param.29) | data formatting | bytes 8388608 | tf_op args[7]
  81.0 0.0 copy-start.5
  81.0 3.4 fusion.8
  84.4 0.1 add_convert_fusion
  84.5 0.1 all_to_all.14
  84.6 0.6 copy.41
  85.2 3.4 all-to-all-start
  88.6 0.0 all-reduce.9.cloned.1.call-start
  88.7 7.0 %all-to-all-done = bf16[2,32,32]{2,0,1:T(2,128)(2,1)S(1)} async-done(((bf16[2,32,32]{2,0,1:T(2,128)(2,1)}), bf16[2,32,32]{2,0,1:T(2,128)(2,1)S(1)}, u32[]{:S(2)}, u32[]{:S(2)}) %all-to-all-start) | async-done | bytes 4128 | tf_op jit(solution)/shard_map/all_to_all | solution.py:117
  95.8 0.0 copy-done.5
  95.8 0.2 fusion.52
  96.0 0.0 copy-done.4
  96.0 0.1 multiply_add_fusion.1
  96.1 0.4 dynamic_update_slice.3
  96.5 0.0 copy-start.2
  96.5 0.8 copy-done.2
  97.3 0.0 all-reduce.9.cloned.1.call-update
  97.3 0.0 all-reduce.11.cloned.1.call-start
  97.4 0.0 copy-done.7
  97.4 0.0 copy-done.8
  97.4 127.8 %all-reduce.9.cloned.1.call-done = f32[64,2048]{1,0:T(8,128)} async-done(((f32[64,2048]{1,0:T(8,128)}), f32[64,2048]{1,0:T(8,128)}) %all-reduce.9.cloned.1.call-update) | async-done | bytes 524304 | tf_op jit(solution)/shard_map/psum | solution.py:121
  225.2 1.2 fusion.44
  226.4 1.2 multiply_convert_fusion
  227.6 0.2 fusion.6
  227.8 0.0 copy-done.6
  227.8 0.2 fusion.53
  228.0 0.0 copy-done.9
  228.1 1.5 fusion.55
  229.6 2.1 fusion.54
  231.7 0.0 copy-done
  231.7 2.5 fusion.1
  234.2 0.0 copy-start.11
  234.2 0.0 copy-start.1
  234.2 3.2 convolution_add_fusion
  237.4 0.0 all-reduce.11.cloned.1.call-update
  237.5 0.0 copy-done.11
  237.5 128.2 %all-reduce.11.cloned.1.call-done = f32[64,2048]{1,0:T(8,128)} async-done(((f32[64,2048]{1,0:T(8,128)}), f32[64,2048]{1,0:T(8,128)}) %all-reduce.11.cloned.1.call-update) | async-done | bytes 524304 | tf_op jit(solution)/shard_map/psum | solution.py:146
  365.7 0.0 copy-done.1
  365.7 1.4 fusion.43
  367.1 0.7 fusion.28
  (19 shorter events, 0.2 us)
Async XLA Ops:
  6.5 225.2 %copy-start = (bf16[512,2048]{1,0:T(8,128)(2,1)S(1)}, bf16[512,2048]{1,0:T(8,128)(2,1)}, u32[]{:S(2)}) copy-start(bf16[512,2048]{1,0:T(8,128)(2,1)} %param.42) | copy-start | bytes 6291460
  65.0 6.2 %copy-start.3 = (f32[2,1024,16]{1,2,0:T(8,128)S(1)}, f32[2,1024,16]{1,2,0:T(8,128)}, u32[]{:S(2)}) copy-start(f32[2,1024,16]{1,2,0:T(8,128)} %param.30) | copy-start | bytes 393220
  71.4 2.9 copy-start.10
  81.0 14.8 %copy-start.5 = (bf16[32,2048]{1,0:T(8,128)(2,1)S(1)}, bf16[32,2048]{1,0:T(8,128)(2,1)}, u32[]{:S(2)}) copy-start(bf16[32,2048]{1,0:T(8,128)(2,1)} %param.32) | copy-start | bytes 393220
  81.0 15.0 %copy-start.4 = (bf16[64,64]{1,0:T(8,128)(2,1)S(1)}, bf16[64,64]{1,0:T(8,128)(2,1)}, u32[]{:S(2)}) copy-start(bf16[64,64]{1,0:T(8,128)(2,1)} %param.22) | copy-start | bytes 24580
  81.0 16.4 %copy-start.7 = (bf16[2048]{0:T(1024)(128)(2,1)S(1)}, bf16[2048]{0:T(1024)(128)(2,1)}, u32[]{:S(2)}) copy-start(bf16[2048]{0:T(1024)(128)(2,1)} %param.33) | copy-start | bytes 12292
  81.0 16.4 %copy-start.8 = (bf16[2048]{0:T(1024)(128)(2,1)S(1)}, bf16[2048]{0:T(1024)(128)(2,1)}, u32[]{:S(2)}) copy-start(bf16[2048]{0:T(1024)(128)(2,1)} %param.36) | copy-start | bytes 12292
  84.4 143.4 %copy-start.6 = (bf16[2048,4]{0,1:T(4,128)(2,1)S(1)}, bf16[2048,4]{0,1:T(4,128)(2,1)}, u32[]{:S(2)}) copy-start(bf16[2048,4]{0,1:T(4,128)(2,1)} %param.34) | copy-start | bytes 49156
  84.4 143.6 %copy-start.9 = (s32[64,2]{0,1:T(2,128)S(1)}, s32[64,2]{0,1:T(2,128)}, u32[]{:S(2)}) copy-start(s32[64,2]{0,1:T(2,128)} %param.35) | copy-start | bytes 1540
  85.2 10.5 %all-to-all-start = ((bf16[2,32,32]{2,0,1:T(2,128)(2,1)}), bf16[2,32,32]{2,0,1:T(2,128)(2,1)S(1)}, u32[]{:S(2)}, u32[]{:S(2)}) async-start(bf16[2,32,32]{2,0,1:T(2,128)(2,1)} %copy.41), calls=%async_computation | async-start | bytes 32768 | tf_op jit(solution)/shard_map/all_to_all | solution.py:117
  88.6 136.6 %all-reduce.9.cloned.1.call-start = ((), (), s32[]{:S(2)}) async-start(), calls=%async_computation.1 | async-start | bytes 1048576 | tf_op jit(solution)/shard_map/psum | solution.py:121
  96.5 0.8 copy-start.2
  97.3 268.4 %all-reduce.11.cloned.1.call-start = ((), (), s32[]{:S(2)}) async-start(), calls=%async_computation.2 | async-start | bytes 1048576 | tf_op jit(solution)/shard_map/psum | solution.py:146
  234.2 3.3 copy-start.11
  234.2 131.5 %copy-start.1 = (f32[64,2048]{1,0:T(8,128)S(1)}, f32[64,2048]{1,0:T(8,128)}, u32[]{:S(2)}) copy-start(f32[64,2048]{1,0:T(8,128)} %all-reduce.9.cloned.1.call-done) | copy-start | bytes 1572868
Sparse Core Ops, SparseCore 0:
  97.4 127.7 all-reduce.8
  237.6 128.0 all-reduce.10
where the time goes:
time: 375 us
  waiting for transfers between devices  263 us (70%)
  blocking collectives  52.3 us (14%)
  matrix products  20.2 us (5%)
  local copies, waits for them, and re-layouts  14.8 us (4%)
  between operations  13.7 us (4%)
  other arithmetic  7.07 us (2%)
    psum x1, waiting for transfers between devices, shards(): branch = lax.psum(local_branch, 'ep')  128 us
    psum x1, waiting for transfers between devices, shards(): lax.psum(lax.dynamic_update_slice_in_dim(partial_sum, placed, offset, 1),...  128 us
    unnamed x1, blocking collectives  52.3 us
    unnamed x27, local copies, waits for them, and re-layouts  13.3 us
  transfers between devices with their start and end apart: 3, of which 3 were waited for; matrix products, arithmetic and copies ran while one was open for 0% of the time, Pallas kernels for 0%

commit v1 on v0

v1 whole, which is shorter than its diff:
```python
import functools

import jax
import jax.numpy as jnp
from jax import lax
from jax.experimental import pallas as pl
from jax.experimental.pallas import tpu as pltpu
from jax.sharding import PartitionSpec as P

norm_eps = 1e-05
residual_scale = 8.0**0.25
MESH = pl.DeviceIdType.MESH
F32 = jnp.float32
BF16 = jnp.bfloat16
LANES = 128
HIGH = lax.Precision.HIGHEST


def iota(shape, dim):
    return lax.broadcasted_iota(jnp.int32, shape, dim)


def dot(a, b):
    return jnp.dot(a, b, preferred_element_type=F32)


def dot_nt(a, b, precision=None):
    return lax.dot_general(
        a, b, (((1,), (1,)), ((), ())), precision=precision, preferred_element_type=F32
    )


def silu(v):
    return v / (1.0 + jnp.exp(-v))


def column_of(row, count):
    shape = (count, row.shape[1])
    hit = iota(shape, 0) == iota(shape, 1)
    return jnp.sum(jnp.where(hit, jnp.broadcast_to(row, shape), 0.0), axis=1, keepdims=True)


def layer_kernel(
    devices,
    lengths,
    tokens,
    w_query,
    w_key,
    w_value,
    w_forget,
    forget_bias,
    w_out,
    norm_gain,
    w_router,
    routes,
    dense_gate,
    final_gain,
    cache_keys,
    cache_values,
    cache_gates,
    expert_w_gate,
    expert_w_up,
    dense_w_gate,
    dense_w_up,
    expert_w_down,
    dense_w_down,
    out,
    keys_v,
    values_v,
    gates_v,
    eg_v,
    eu_v,
    dg_v,
    du_v,
    ed_v,
    dd_v,
    proj,
    proj_in,
    reduced,
    qkv,
    forget,
    forget_in,
    tok_own,
    tok_pair,
    wcol,
    attn_f,
    attn_own,
    attn_in,
    mixed_own,
    mixed_all,
    normed_v,
    branch_v,
    branch_in,
    fin_own,
    fin_pair,
    stat_own,
    stat_in,
    local_sem,
    send_sem,
    recv_sem,
    pair_sem,
):
    me = lax.axis_index("ep")
    seqs, feat = tokens.shape
    seqs_here, cache_len, width = cache_keys.shape
    heads = cache_gates.shape[2]
    head_size = width // heads
    model = norm_gain.shape[1]
    experts = w_router.shape[1]
    rows_f = forget_in.shape[1]
    rows_p = proj_in.shape[1]
    cols_p = proj_in.shape[2]
    members = devices // (seqs // rows_p)
    per_f = rows_f // seqs_here
    half = seqs // 2
    pair = me // 2
    side = me % 2
    partner = 2 * pair + 1 - side
    block = 2 * feat

    barrier = pltpu.get_barrier_semaphore()

    def greet(step, carry):
        pl.semaphore_signal(
            barrier, inc=1, device_id={"ep": (me + step) % devices}, device_id_type=MESH
        )
        return carry

    lax.fori_loop(1, devices, greet, 0)

    big = (
        (cache_gates, gates_v),
        (cache_keys, keys_v),
        (cache_values, values_v),
        (expert_w_gate, eg_v),
        (expert_w_up, eu_v),
        (dense_w_gate, dg_v),
        (dense_w_up, du_v),
        (expert_w_down, ed_v),
        (dense_w_down, dd_v),
    )
    loads = [
        pltpu.make_async_copy(src, dst, local_sem.at[i]) for i, (src, dst) in enumerate(big)
    ]
    for load in loads:
        load.start()

    def remote(phase, src, dst, dest, slot, origin):
        return pltpu.make_async_remote_copy(
            src_ref=src,
            dst_ref=dst,
            send_sem=send_sem.at[phase, slot],
            recv_sem=recv_sem.at[phase, origin],
            device_id={"ep": dest},
            device_id_type=MESH,
        )

    def each(count, mine, fn):
        def body(step, carry):
            fn((mine + step) % count)
            return carry

        lax.fori_loop(1, count, body, 0)

    x = tokens[...]
    proj[:, 0:width] = dot(x, w_query[...]).astype(BF16)
    proj[:, width : 2 * width] = dot(x, w_key[...]).astype(BF16)
    proj[:, 2 * width : 3 * width] = dot(x, w_value[...]).astype(BF16)
    forget[...] = jnp.zeros_like(forget)
    forget[:, 0:heads] = dot(x, w_forget[...])
    place = (iota((feat, block), 1) == iota((feat, block), 0) + side * feat).astype(BF16)
    tok_own[...] = dot(x, place).astype(BF16)

    pl.semaphore_wait(barrier, devices - 1)

    def proj_src(d):
        return proj.at[
            pl.ds(pl.multiple_of(rows_p * (d // members), rows_p), rows_p),
            pl.ds(pl.multiple_of(cols_p * (d % members), LANES), cols_p),
        ]

    def forget_src(d):
        return forget.at[pl.ds(pl.multiple_of(rows_f * (d // per_f), rows_f), rows_f)]

    def wout_src(d):
        return w_out.at[:, pl.ds(pl.multiple_of(block * (d // 2), LANES), block)]

    def copy_proj(d, origin):
        return remote(0, proj_src(d), proj_in.at[origin], d, d, origin)

    def copy_forget(d, origin):
        return remote(1, forget_src(d), forget_in.at[origin], d, d, origin)

    def copy_wout(d, origin):
        return remote(2, wout_src(d), wcol.at[origin], d, d, origin)

    each(devices, me, lambda d: copy_proj(d, me).start())
    each(devices, me, lambda d: copy_forget(d, me).start())
    each(devices, me, lambda d: copy_wout(d, me).start())
    tok_copy = pltpu.make_async_remote_copy(
        src_ref=tok_own,
        dst_ref=tok_pair,
        send_sem=pair_sem.at[0],
        recv_sem=pair_sem.at[1],
        device_id={"ep": partner},
        device_id_type=MESH,
    )
    tok_copy.start()

    proj_in[me] = proj[
        pl.ds(pl.multiple_of(rows_p * (me // members), rows_p), rows_p),
        pl.ds(pl.multiple_of(cols_p * (me % members), LANES), cols_p),
    ]
    forget_in[me] = forget[pl.ds(pl.multiple_of(rows_f * (me // per_f), rows_f), rows_f), :]
    wcol[me] = w_out[:, pl.ds(pl.multiple_of(block * pair, LANES), block)]

    loads[0].wait()
    eye = (iota((heads, heads), 0) == iota((heads, heads), 1)).astype(F32)
    position = iota((heads, cache_len), 1)
    gates_t = []
    for b in range(seqs_here):
        turned = dot_nt(eye, gates_v[b], HIGH)
        last = jnp.sum(
            jnp.where(position == lengths[b] - 1, turned, 0.0), axis=1, keepdims=True
        )
        gates_t.append(last - turned)

    each(devices, me, lambda d: copy_proj(d, d).wait_recv())
    total = proj_in[0].astype(F32)
    for s in range(1, devices):
        total = total + proj_in[s].astype(F32)
    reduced[...] = total.astype(BF16)

    group = me // members
    member = me % members

    def qkv_slot(m):
        return qkv.at[:, pl.ds(pl.multiple_of(cols_p * m, LANES), cols_p)]

    def copy_group(m, origin):
        return remote(3, reduced, qkv_slot(origin), group * members + m, m, origin)

    each(members, member, lambda m: copy_group(m, member).start())
    qkv[:, pl.ds(pl.multiple_of(cols_p * member, LANES), cols_p)] = total.astype(BF16)

    each(devices, me, lambda d: copy_forget(d, d).wait_recv())
    forget_sum = forget_in[0]
    for s in range(1, devices):
        forget_sum = forget_sum + forget_in[s]

    each(members, member, lambda m: copy_group(m, m).wait_recv())
    mine = qkv[...].astype(F32)
    scale = head_size ** (-0.5)
    diagonal = iota((heads, width), 1) // head_size == iota((heads, width), 0)
    loads[1].wait()
    loads[2].wait()
    for b in range(seqs_here):
        at_p = iota(mine.shape, 0) == seqs_here * member + b
        row = jnp.sum(jnp.where(at_p, mine, 0.0), axis=0, keepdims=True)
        at_f = iota(forget_sum.shape, 0) == seqs_here * (me % per_f) + b
        pre = jnp.sum(jnp.where(at_f, forget_sum, 0.0), axis=0, keepdims=True)
        pre = column_of(pre, heads) + column_of(forget_bias[...], heads)
        log_gate = jnp.minimum(pre, 0.0) - jnp.log(1.0 + jnp.exp(-jnp.abs(pre)))
        query = jnp.where(diagonal, row[:, 0:width], 0.0)
        own_score = jnp.sum(query * row[:, width : 2 * width], axis=1, keepdims=True) * scale
        scores = dot_nt(query.astype(BF16), keys_v[b]) * scale + (gates_t[b] + log_gate)
        scores = jnp.where(position < lengths[b], scores, -jnp.inf)
        top = jnp.maximum(jnp.max(scores, axis=1, keepdims=True), own_score)
        weights = jnp.exp(scores - top)
        own = jnp.exp(own_score - top)
        total_w = jnp.sum(weights, axis=1, keepdims=True) + own
        probs = (weights / total_w).astype(BF16)
        own = (own / total_w).astype(BF16).astype(F32)
        seen = dot(probs, values_v[b]) + own * row[:, 2 * width : 3 * width]
        attn_row = jnp.sum(jnp.where(diagonal, seen, 0.0), axis=0, keepdims=True)
        for j in range(width // LANES):
            at = b * (width // LANES) + j
            attn_f[at : at + 1, :] = attn_row[:, j * LANES : (j + 1) * LANES]
    attn_own[...] = attn_f[...].astype(BF16)

    def copy_attn(d, origin):
        return remote(4, attn_own, attn_in.at[origin], d, d, origin)

    each(devices, me, lambda d: copy_attn(d, me).start())
    attn_in[me] = attn_own[...]
    tok_copy.wait_recv()
    residual = residual_scale * (tok_own[...].astype(F32) + tok_pair[...].astype(F32))
    each(devices, me, lambda d: copy_wout(d, d).wait_recv())
    each(devices, me, lambda d: copy_attn(d, d).wait_recv())

    pieces = width // LANES
    attn_all = attn_in[...].reshape(seqs * pieces, LANES)
    w_cols = wcol[...].reshape(width, block)
    acc = jnp.zeros((seqs * pieces, block), F32)
    turn = iota((seqs * pieces, block), 0) % pieces
    for j in range(pieces):
        part = dot(attn_all, w_cols[j * LANES : (j + 1) * LANES, :])
        acc = jnp.where(turn == j, part, acc)
    mixed = residual + jnp.sum(acc.reshape(seqs, pieces, block), axis=1)
    mixed_own[...] = mixed.astype(BF16)

    def copy_mixed(k, origin):
        return remote(
            5,
            mixed_own,
            mixed_all.at[:, pl.ds(pl.multiple_of(block * origin, LANES), block)],
            2 * k + side,
            k,
            origin,
        )

    pairs = devices // 2
    each(pairs, pair, lambda k: copy_mixed(k, pair).start())
    mixed_all[:, pl.ds(pl.multiple_of(block * pair, LANES), block)] = mixed.astype(BF16)
    each(pairs, pair, lambda k: copy_mixed(k, k).wait_recv())

    mixed = mixed_all[...].astype(F32)
    center = jnp.mean(mixed, axis=1, keepdims=True)
    second = jnp.mean(mixed * mixed, axis=1, keepdims=True)
    normed = (
        (mixed - center)
        * lax.rsqrt(second - center * center + norm_eps)
        * norm_gain[...].astype(F32)
    ).astype(BF16)
    normed_v[...] = normed

    logits = dot(normed, w_router[...])
    first, other = routes[:, 0:1], routes[:, 1:2]
    shape = logits.shape
    chosen_a = jnp.sum(jnp.where(iota(shape, 1) == first, logits, 0.0), axis=1, keepdims=True)
    chosen_b = jnp.sum(jnp.where(iota(shape, 1) == other, logits, 0.0), axis=1, keepdims=True)
    top = jnp.maximum(chosen_a, chosen_b)
    exp_a, exp_b = jnp.exp(chosen_a - top), jnp.exp(chosen_b - top)
    expert = me // (devices // experts)
    share = (
        jnp.where(first == expert, exp_a, 0.0) + jnp.where(other == expert, exp_b, 0.0)
    ) / (exp_a + exp_b)
    dense_pre = jnp.sum(
        normed.astype(F32) * dense_gate[...].astype(F32), axis=1, keepdims=True
    )
    dense_scale = 1.0 / (1.0 + jnp.exp(-dense_pre))

    loads[3].wait()
    loads[4].wait()
    hidden_e = (share * silu(dot(normed, eg_v[...])) * dot(normed, eu_v[...])).astype(BF16)
    loads[5].wait()
    loads[6].wait()
    hidden_d = (dense_scale * silu(dot(normed, dg_v[...])) * dot(normed, du_v[...])).astype(BF16)
    loads[7].wait()
    loads[8].wait()
    branch_v[...] = (dot(hidden_e, ed_v[...]) + dot(hidden_d, dd_v[...])).astype(BF16)

    def branch_at(d):
        return (
            pl.ds(pl.multiple_of(half * (d % 2), half), half),
            pl.ds(pl.multiple_of(block * (d // 2), LANES), block),
        )

    def copy_branch(d, origin):
        return remote(6, branch_v.at[branch_at(d)], branch_in.at[origin], d, d, origin)

    each(devices, me, lambda d: copy_branch(d, me).start())
    branch_in[me] = branch_v[branch_at(me)]
    each(devices, me, lambda d: copy_branch(d, d).wait_recv())
    final = residual_scale * normed_v[branch_at(me)].astype(F32)
    for s in range(devices):
        final = final + branch_in[s].astype(F32)
    fin_own[...] = final
    fin_copy = pltpu.make_async_remote_copy(
        src_ref=fin_own,
        dst_ref=fin_pair,
        send_sem=pair_sem.at[2],
        recv_sem=pair_sem.at[3],
        device_id={"ep": partner},
        device_id_type=MESH,
    )
    fin_copy.start()
    ones = jnp.ones((stat_own.shape[0], block), F32)
    sums = dot_nt(ones, final, HIGH)
    squares = dot_nt(ones, final * final, HIGH)
    stat_own[...] = jnp.zeros_like(stat_own)
    stat_own[:, 0:half] = jnp.where(iota(sums.shape, 0) == 0, sums, squares)

    def copy_stat(d, origin):
        return remote(7, stat_own, stat_in.at[origin], d, d, origin)

    each(devices, me, lambda d: copy_stat(d, me).start())
    stat_in[me] = stat_own[...]
    fin_copy.wait_recv()
    each(devices, me, lambda d: copy_stat(d, d).wait_recv())

    other_final = fin_pair[...]
    gain = final_gain[...].astype(F32)
    for p in range(2):
        stat = stat_in[p]
        for s in range(p + 2, devices, 2):
            stat = stat + stat_in[s]
        center = column_of(stat[0:1, :], half) / model
        second = column_of(stat[1:2, :], half) / model
        value = jnp.where(side == p, final, other_final)
        unit = (value - center) * lax.rsqrt(second - center * center + norm_eps)
        unit = jnp.where(side == 0, unit, pltpu.roll(unit, feat, 1))
        out[p * half : (p + 1) * half, :] = (unit[:, 0:feat] * gain).astype(BF16)

    each(devices, me, lambda d: copy_proj(d, me).wait_send())
    each(devices, me, lambda d: copy_forget(d, me).wait_send())
    each(devices, me, lambda d: copy_wout(d, me).wait_send())
    each(members, member, lambda m: copy_group(m, member).wait_send())
    each(devices, me, lambda d: copy_attn(d, me).wait_send())
    each(pairs, pair, lambda k: copy_mixed(k, pair).wait_send())
    each(devices, me, lambda d: copy_branch(d, me).wait_send())
    each(devices, me, lambda d: copy_stat(d, me).wait_send())
    tok_copy.wait_send()
    fin_copy.wait_send()


def shards(
    devices,
    tokens,
    w_query,
    w_key,
    w_value,
    w_forget,
    forget_bias,
    cache_keys,
    cache_values,
    cache_gates,
    lengths,
    w_out,
    norm_gain,
    w_router,
    routes,
    dense_gate,
    dense_w_gate,
    dense_w_up,
    dense_w_down,
    expert_w_gate,
    expert_w_up,
    expert_w_down,
    final_gain,
):
    seqs, feat = tokens.shape
    seqs_here, cache_len, width = cache_keys.shape
    model = norm_gain.shape[0]
    rows_p, rows_f = 16, 8
    members = devices // (seqs // rows_p)
    cols_p = 3 * width // members
    block = 2 * feat
    half = seqs // 2
    pieces = width // LANES
    vmem = pl.BlockSpec(memory_space=pltpu.VMEM)
    hbm = pl.BlockSpec(memory_space=pl.ANY)
    big = (
        cache_keys,
        cache_values,
        cache_gates,
        expert_w_gate,
        expert_w_up,
        dense_w_gate,
        dense_w_up,
        expert_w_down,
        dense_w_down,
    )
    return pl.pallas_call(
        functools.partial(layer_kernel, devices),
        out_shape=jax.ShapeDtypeStruct((seqs, feat), BF16),
        in_specs=[pl.BlockSpec(memory_space=pltpu.SMEM)] + [vmem] * 12 + [hbm] * len(big),
        out_specs=vmem,
        scratch_shapes=[pltpu.VMEM(a.shape, a.dtype) for a in big]
        + [
            pltpu.VMEM((seqs, 3 * width), BF16),
            pltpu.VMEM((devices, rows_p, cols_p), BF16),
            pltpu.VMEM((rows_p, cols_p), BF16),
            pltpu.VMEM((rows_p, 3 * width), BF16),
            pltpu.VMEM((seqs, LANES), F32),
            pltpu.VMEM((devices, rows_f, LANES), F32),
            pltpu.VMEM((seqs, block), BF16),
            pltpu.VMEM((seqs, block), BF16),
            pltpu.VMEM((devices, width // devices, block), BF16),
            pltpu.VMEM((seqs_here * pieces, LANES), F32),
            pltpu.VMEM((seqs_here * pieces, LANES), BF16),
            pltpu.VMEM((devices, seqs_here * pieces, LANES), BF16),
            pltpu.VMEM((seqs, block), BF16),
            pltpu.VMEM((seqs, model), BF16),
            pltpu.VMEM((seqs, model), BF16),
            pltpu.VMEM((seqs, model), BF16),
            pltpu.VMEM((devices, half, block), BF16),
            pltpu.VMEM((half, block), F32),
            pltpu.VMEM((half, block), F32),
            pltpu.VMEM((8, LANES), F32),
            pltpu.VMEM((devices, 8, LANES), F32),
            pltpu.SemaphoreType.DMA((len(big),)),
            pltpu.SemaphoreType.DMA((8, devices)),
            pltpu.SemaphoreType.DMA((8, devices)),
            pltpu.SemaphoreType.DMA((4,)),
        ],
        compiler_params=pltpu.CompilerParams(
            collective_id=0, has_side_effects=True, vmem_limit_bytes=60 * 1024 * 1024
        ),
    )(
        lengths,
        tokens,
        w_query,
        w_key,
        w_value,
        w_forget,
        forget_bias[None, :],
        w_out,
        norm_gain[None, :],
        w_router,
        routes,
        dense_gate[None, :],
        final_gain[None, :],
        *big,
    )


def solution(mesh):
    placed = (
        P("grp", "ep"),
        P("ep", None),
        P("ep", None),
        P("ep", None),
        P("ep", None),
        P(),
        P(("grp", "ep"), None, None),
        P(("grp", "ep"), None, None),
        P(("grp", "ep"), None, None),
        P(("grp", "ep")),
        P("ep", None),
        P(),
        P(),
        P("grp", None),
        P(),
        P(None, "ep"),
        P(None, "ep"),
        P("ep", None),
        P(None, "ep"),
        P(None, "ep"),
        P("ep", None),
        P("ep"),
    )
    return jax.shard_map(
        functools.partial(shards, mesh.shape["ep"]),
        mesh=mesh,
        in_specs=placed,
        out_specs=P("grp", "ep"),
        check_vma=False,
    )
```

time: 375 us -> 75.5 us (0.20)
  waiting for transfers between devices: 263 us -> 0 us
  Pallas kernels: 0 us -> 64.4 us
  blocking collectives: 52.3 us -> 0 us
  matrix products: 20.2 us -> 0 us
  between operations: 13.7 us -> 0.01 us
  other arithmetic: 7.07 us -> 0 us
  local copies, waits for them, and re-layouts: 14.8 us -> 10.7 us
    psum x2 -> x0, waiting for transfers between devices: 256 us -> none  [the longest x1 128 us: shards(): branch = lax.psum(local_branch, 'ep')]
    pallas_call x0 -> x1, Pallas kernels: none -> 64.4 us  [shards(): pl.pallas_call(functools.partial(layer_kernel, devices), out_shape=jax.Sh...]
    unnamed x1 -> x0, blocking collectives: 52.3 us -> none
    dot_general x13 -> x0, matrix products: 20.2 us -> none  [the longest x1 3.4 us: attend(): jnp.einsum('shl,slhd->shd', probs, values_all, preferred_element_type=jnp...]
    all_to_all x1 -> x0, waiting for transfers between devices: 7.05 us -> none  [shards(): lax.all_to_all(attn, 'ep', split_axis=1, concat_axis=0, tiled=True)]
    unnamed x27 -> x5, local copies, waits for them, and re-layouts: 13.3 us -> 8.09 us
  transfers between devices with their start and end apart: 3 -> 0, of which waited for: 3 -> 0; matrix products, arithmetic and copies ran while one was open for 0% -> 0% of each run, Pallas kernels for 0% -> 0%
where the time goes in v1:
time: 75.5 us; the launch traced here: 75.1 us
  Pallas kernels  64.4 us (85%)
  local copies, waits for them, and re-layouts  10.7 us (14%)
    pallas_call x1, Pallas kernels, shards(): pl.pallas_call(functools.partial(layer_kernel, devices), out_shape=jax.Sh...  64.4 us
    unnamed x5, local copies, waits for them, and re-layouts  8.09 us

profile of v1, /device:TPU:0, one launch (start us, length us, event | category | flops | bytes accessed | tf_op | source)
XLA Modules:
  0.0 75.1 jit_solution(13359423501707962995)
XLA Ops:
  0.0 1.3 %broadcast_in_dim.13.norm_gain = bf16[1,2048]{1,0:T(2,128)(2,1)} reshape(bf16[2048]{0:T(1024)(128)(2,1)} %param.33) | data formatting | bytes 8192 | tf_op jit(solution)/shard_map/broadcast_in_dim | solution.py:509
  1.3 1.3 %broadcast_in_dim.14.dense_gate = bf16[1,2048]{1,0:T(2,128)(2,1)} reshape(bf16[2048]{0:T(1024)(128)(2,1)} %param.36) | data formatting | bytes 8192 | tf_op jit(solution)/shard_map/broadcast_in_dim | solution.py:512
  2.6 1.4 %copy.23.w_forget = bf16[64,16]{1,0:T(8,128)(2,1)} copy(bf16[64,16]{0,1:T(8,128)(2,1)} %param.26) | data formatting | bytes 4096 | tf_op args[4]
  3.9 1.4 %copy.25.routes = s32[64,2]{1,0:T(8,128)} copy(s32[64,2]{0,1:T(2,128)} %param.35) | data formatting | bytes 1024 | tf_op args[13]
  5.3 1.8 %copy.24.w_router = bf16[2048,4]{1,0:T(8,128)(2,1)} copy(bf16[2048,4]{0,1:T(4,128)(2,1)} %param.34) | data formatting | bytes 32768 | tf_op args[12]
  7.1 2.2 %copy.26.cache_gates = f32[2,1024,16]{2,1,0:T(8,128)} copy(f32[2,1024,16]{1,2,0:T(8,128)} %param.30) | data formatting | bytes 262144 | tf_op args[8]
  9.3 64.4 %shard_map.208 = bf16[64,64]{1,0:T(8,128)(2,1)} custom-call(s32[2]{0:T(128)} %lengths.1, bf16[64,64]{1,0:T(8,128)(2,1)} %tokens.1, bf16[64,1024]{1,0:T(8,128)(2,1)} %w_query.1, bf16[64,1024]{1,0:T(8,128)(2,1)} %w_key.1, bf16[64,1024]{1,0:T(8,128)(2,1)} %w_value.1, bf16[64,16]{1,0:T(8,128)(2,1)} %copy.23.w_forget, f32[1,16]{1,0:T(1,128)} %bitcast.2, ...), custom_call_target="tpu_custom_call" | custom-call | tf_op jit(solution)/shard_map/pallas_call | solution.py:464
  73.7 1.3 %copy.28 = bf16[64,64]{1,0:T(8,128)(2,1)} copy(bf16[64,64]{1,0:T(8,128)(2,1)} %shard_map.208) | data formatting | bytes 16384

commit v2 on v1

--- a/solution.py
+++ b/solution.py
@@ -34,10 +34,15 @@
     return v / (1.0 + jnp.exp(-v))
 
 
-def column_of(row, count):
+def column_of(row, count, start=0):
     shape = (count, row.shape[1])
-    hit = iota(shape, 0) == iota(shape, 1)
+    hit = iota(shape, 0) + start == iota(shape, 1)
     return jnp.sum(jnp.where(hit, jnp.broadcast_to(row, shape), 0.0), axis=1, keepdims=True)
+
+
+def row_of(tile):
+    tile = tile.astype(F32)
+    return jnp.concatenate([tile[i : i + 1, :] for i in range(tile.shape[0])], axis=1)
 
 
 def layer_kernel(
@@ -75,11 +80,14 @@
     ed_v,
     dd_v,
     proj,
+    proj_pair,
+    proj_sum,
     proj_in,
     reduced,
     qkv,
     forget,
     forget_in,
+    forget_quad,
     tok_own,
     tok_pair,
     wcol,
@@ -90,6 +98,8 @@
     mixed_all,
     normed_v,
     branch_v,
+    branch_pair,
+    branch_sum,
     branch_in,
     fin_own,
     fin_pair,
@@ -103,10 +113,10 @@
     me = lax.axis_index("ep")
     seqs, feat = tokens.shape
     seqs_here, cache_len, width = cache_keys.shape
-    heads = cache_gates.shape[2]
+    heads = cache_gates.shape[1]
     head_size = width // heads
-    model = norm_gain.shape[1]
-    experts = w_router.shape[1]
+    model = mixed_all.shape[1]
+    experts = w_router.shape[0]
     rows_f = forget_in.shape[1]
     rows_p = proj_in.shape[1]
     cols_p = proj_in.shape[2]
@@ -117,6 +127,13 @@
     side = me % 2
     partner = 2 * pair + 1 - side
     block = 2 * feat
+    pairs = devices // 2
+    side_w = proj_pair.shape[1]
+    groups_f = seqs // rows_f
+    group = me // members
+    member = me % members
+    group_f = me // per_f
+    member_f = me % per_f
 
     barrier = pltpu.get_barrier_semaphore()
 
@@ -167,86 +184,113 @@
     proj[:, width : 2 * width] = dot(x, w_key[...]).astype(BF16)
     proj[:, 2 * width : 3 * width] = dot(x, w_value[...]).astype(BF16)
     forget[...] = jnp.zeros_like(forget)
-    forget[:, 0:heads] = dot(x, w_forget[...])
+    forget[:, 0:heads] = dot_nt(x, w_forget[...])
     place = (iota((feat, block), 1) == iota((feat, block), 0) + side * feat).astype(BF16)
     tok_own[...] = dot(x, place).astype(BF16)
 
     pl.semaphore_wait(barrier, devices - 1)
 
-    def proj_src(d):
-        return proj.at[
+    def pair_copy(i, src, dst):
+        return pltpu.make_async_remote_copy(
+            src_ref=src,
+            dst_ref=dst,
+            send_sem=pair_sem.at[2 * i],
+            recv_sem=pair_sem.at[2 * i + 1],
+            device_id={"ep": partner},
+            device_id_type=MESH,
+        )
+
+    def side_cols(at):
+        return pl.ds(pl.multiple_of(side_w * at, LANES), side_w)
+
+    def block_cols(k):
+        return pl.ds(pl.multiple_of(block * k, LANES), block)
+
+    def piece(m):
+        return (m % 2) * (members // 2) + m // 2
+
+    def proj_at(k):
+        d = 2 * k + side
+        return (
             pl.ds(pl.multiple_of(rows_p * (d // members), rows_p), rows_p),
-            pl.ds(pl.multiple_of(cols_p * (d % members), LANES), cols_p),
-        ]
-
-    def forget_src(d):
-        return forget.at[pl.ds(pl.multiple_of(rows_f * (d // per_f), rows_f), rows_f)]
-
-    def wout_src(d):
-        return w_out.at[:, pl.ds(pl.multiple_of(block * (d // 2), LANES), block)]
-
-    def copy_proj(d, origin):
-        return remote(0, proj_src(d), proj_in.at[origin], d, d, origin)
-
-    def copy_forget(d, origin):
-        return remote(1, forget_src(d), forget_in.at[origin], d, d, origin)
-
-    def copy_wout(d, origin):
-        return remote(2, wout_src(d), wcol.at[origin], d, d, origin)
-
-    each(devices, me, lambda d: copy_proj(d, me).start())
-    each(devices, me, lambda d: copy_forget(d, me).start())
-    each(devices, me, lambda d: copy_wout(d, me).start())
-    tok_copy = pltpu.make_async_remote_copy(
-        src_ref=tok_own,
-        dst_ref=tok_pair,
-        send_sem=pair_sem.at[0],
-        recv_sem=pair_sem.at[1],
-        device_id={"ep": partner},
-        device_id_type=MESH,
-    )
+            pl.ds(pl.multiple_of(cols_p * ((d % members) // 2), LANES), cols_p),
+        )
+
+    def forget_at(g):
+        return pl.ds(pl.multiple_of(rows_f * g, rows_f), rows_f)
+
+    def copy_proj(k, origin):
+        return remote(0, proj_sum.at[proj_at(k)], proj_in.at[origin], 2 * k + side, k, origin)
+
+    def copy_forget(g, origin):
+        return remote(
+            1, forget.at[forget_at(g)], forget_in.at[origin], per_f * g + member_f, g, origin
+        )
+
+    def copy_wout(k, origin):
+        return remote(
+            2, w_out.at[:, block_cols(k)], wcol.at[origin, side], 2 * k + side, k, origin
+        )
+
+    proj_copy = pair_copy(2, proj.at[:, side_cols(1 - side)], proj_pair)
+    proj_copy.start()
+    each(groups_f, group_f, lambda g: copy_forget(g, group_f).start())
+    tok_copy = pair_copy(0, tok_own, tok_pair)
     tok_copy.start()
-
-    proj_in[me] = proj[
-        pl.ds(pl.multiple_of(rows_p * (me // members), rows_p), rows_p),
-        pl.ds(pl.multiple_of(cols_p * (me % members), LANES), cols_p),
-    ]
-    forget_in[me] = forget[pl.ds(pl.multiple_of(rows_f * (me // per_f), rows_f), rows_f), :]
-    wcol[me] = w_out[:, pl.ds(pl.multiple_of(block * pair, LANES), block)]
+    forget_in[group_f] = forget[forget_at(group_f), :]
+    proj_copy.wait_recv()
+    proj_sum[...] = (
+        proj[:, side_cols(side)].astype(F32) + proj_pair[...].astype(F32)
+    ).astype(BF16)
+    each(pairs, pair, lambda k: copy_proj(k, pair).start())
+    proj_in[pair] = proj_sum[proj_at(pair)]
+    wcol[pair, side] = w_out[:, block_cols(pair)]
+
+    each(groups_f, group_f, lambda g: copy_forget(g, g).wait_recv())
+    forget_sum = forget_in[0]
+    for g in range(1, groups_f):
+        forget_sum = forget_sum + forget_in[g]
+    forget_quad[member_f] = forget_sum
+
+    def copy_quad(m, origin):
+        return remote(
+            8, forget_quad.at[member_f], forget_quad.at[origin], per_f * group_f + m, m, origin
+        )
+
+    each(per_f, member_f, lambda m: copy_quad(m, member_f).start())
 
     loads[0].wait()
-    eye = (iota((heads, heads), 0) == iota((heads, heads), 1)).astype(F32)
     position = iota((heads, cache_len), 1)
     gates_t = []
     for b in range(seqs_here):
-        turned = dot_nt(eye, gates_v[b], HIGH)
+        turned = gates_v[b]
         last = jnp.sum(
             jnp.where(position == lengths[b] - 1, turned, 0.0), axis=1, keepdims=True
         )
         gates_t.append(last - turned)
 
-    each(devices, me, lambda d: copy_proj(d, d).wait_recv())
+    each(pairs, pair, lambda k: copy_proj(k, k).wait_recv())
     total = proj_in[0].astype(F32)
-    for s in range(1, devices):
+    for s in range(1, pairs):
         total = total + proj_in[s].astype(F32)
     reduced[...] = total.astype(BF16)
 
-    group = me // members
-    member = me % members
-
-    def qkv_slot(m):
-        return qkv.at[:, pl.ds(pl.multiple_of(cols_p * m, LANES), cols_p)]
+    def qkv_cols(m):
+        return pl.ds(pl.multiple_of(cols_p * piece(m), LANES), cols_p)
 
     def copy_group(m, origin):
-        return remote(3, reduced, qkv_slot(origin), group * members + m, m, origin)
+        return remote(
+            3, reduced, qkv.at[:, qkv_cols(origin)], group * members + m, m, origin
+        )
 
     each(members, member, lambda m: copy_group(m, member).start())
-    qkv[:, pl.ds(pl.multiple_of(cols_p * member, LANES), cols_p)] = total.astype(BF16)
-
-    each(devices, me, lambda d: copy_forget(d, d).wait_recv())
-    forget_sum = forget_in[0]
-    for s in range(1, devices):
-        forget_sum = forget_sum + forget_in[s]
+    each(pairs, pair, lambda k: copy_wout(k, pair).start())
+    qkv[:, qkv_cols(member)] = total.astype(BF16)
+
+    each(per_f, member_f, lambda m: copy_quad(m, m).wait_recv())
+    forget_sum = forget_quad[0]
+    for m in range(1, per_f):
+        forget_sum = forget_sum + forget_quad[m]
 
     each(members, member, lambda m: copy_group(m, m).wait_recv())
     mine = qkv[...].astype(F32)
@@ -257,7 +301,7 @@
     for b in range(seqs_here):
         at_p = iota(mine.shape, 0) == seqs_here * member + b
         row = jnp.sum(jnp.where(at_p, mine, 0.0), axis=0, keepdims=True)
-        at_f = iota(forget_sum.shape, 0) == seqs_here * (me % per_f) + b
+        at_f = iota(forget_sum.shape, 0) == seqs_here * member_f + b
         pre = jnp.sum(jnp.where(at_f, forget_sum, 0.0), axis=0, keepdims=True)
         pre = column_of(pre, heads) + column_of(forget_bias[...], heads)
         log_gate = jnp.minimum(pre, 0.0) - jnp.log(1.0 + jnp.exp(-jnp.abs(pre)))
@@ -285,7 +329,10 @@
     attn_in[me] = attn_own[...]
     tok_copy.wait_recv()
     residual = residual_scale * (tok_own[...].astype(F32) + tok_pair[...].astype(F32))
-    each(devices, me, lambda d: copy_wout(d, d).wait_recv())
+    each(pairs, pair, lambda k: copy_wout(k, k).wait_recv())
+    wout_copy = pair_copy(3, wcol.at[:, side], wcol.at[:, side])
+    wout_copy.start()
+    wout_copy.wait_recv()
     each(devices, me, lambda d: copy_attn(d, d).wait_recv())
 
     pieces = width // LANES
@@ -303,15 +350,14 @@
         return remote(
             5,
             mixed_own,
-            mixed_all.at[:, pl.ds(pl.multiple_of(block * origin, LANES), block)],
+            mixed_all.at[:, block_cols(origin)],
             2 * k + side,
             k,
             origin,
         )
 
-    pairs = devices // 2
     each(pairs, pair, lambda k: copy_mixed(k, pair).start())
-    mixed_all[:, pl.ds(pl.multiple_of(block * pair, LANES), block)] = mixed.astype(BF16)
+    mixed_all[:, block_cols(pair)] = mixed.astype(BF16)
     each(pairs, pair, lambda k: copy_mixed(k, k).wait_recv())
 
     mixed = mixed_all[...].astype(F32)
@@ -320,12 +366,14 @@
     normed = (
         (mixed - center)
         * lax.rsqrt(second - center * center + norm_eps)
-        * norm_gain[...].astype(F32)
+        * row_of(norm_gain[...])
     ).astype(BF16)
     normed_v[...] = normed
 
-    logits = dot(normed, w_router[...])
-    first, other = routes[:, 0:1], routes[:, 1:2]
+    logits = dot_nt(normed, w_router[...])
+    names = routes[...].astype(F32)
+    first = column_of(names[0:1, :], seqs).astype(jnp.int32)
+    other = column_of(names[1:2, :], seqs).astype(jnp.int32)
     shape = logits.shape
     chosen_a = jnp.sum(jnp.where(iota(shape, 1) == first, logits, 0.0), axis=1, keepdims=True)
     chosen_b = jnp.sum(jnp.where(iota(shape, 1) == other, logits, 0.0), axis=1, keepdims=True)
@@ -336,7 +384,7 @@
         jnp.where(first == expert, exp_a, 0.0) + jnp.where(other == expert, exp_b, 0.0)
     ) / (exp_a + exp_b)
     dense_pre = jnp.sum(
-        normed.astype(F32) * dense_gate[...].astype(F32), axis=1, keepdims=True
+        normed.astype(F32) * row_of(dense_gate[...]), axis=1, keepdims=True
     )
     dense_scale = 1.0 / (1.0 + jnp.exp(-dense_pre))
 
@@ -350,36 +398,36 @@
     loads[8].wait()
     branch_v[...] = (dot(hidden_e, ed_v[...]) + dot(hidden_d, dd_v[...])).astype(BF16)
 
-    def branch_at(d):
-        return (
-            pl.ds(pl.multiple_of(half * (d % 2), half), half),
-            pl.ds(pl.multiple_of(block * (d // 2), LANES), block),
-        )
-
-    def copy_branch(d, origin):
-        return remote(6, branch_v.at[branch_at(d)], branch_in.at[origin], d, d, origin)
-
-    each(devices, me, lambda d: copy_branch(d, me).start())
-    branch_in[me] = branch_v[branch_at(me)]
-    each(devices, me, lambda d: copy_branch(d, d).wait_recv())
-    final = residual_scale * normed_v[branch_at(me)].astype(F32)
-    for s in range(devices):
+    def half_rows(at):
+        return pl.ds(pl.multiple_of(half * at, half), half)
+
+    branch_copy = pair_copy(4, branch_v.at[half_rows(1 - side)], branch_pair)
+    branch_copy.start()
+    final = residual_scale * normed_v[half_rows(side), block_cols(pair)].astype(F32)
+    branch_copy.wait_recv()
+    branch_sum[...] = (
+        branch_v[half_rows(side), :].astype(F32) + branch_pair[...].astype(F32)
+    ).astype(BF16)
+
+    def copy_branch(k, origin):
+        return remote(
+            6, branch_sum.at[:, block_cols(k)], branch_in.at[origin], 2 * k + side, k, origin
+        )
+
+    each(pairs, pair, lambda k: copy_branch(k, pair).start())
+    branch_in[pair] = branch_sum[:, block_cols(pair)]
+    each(pairs, pair, lambda k: copy_branch(k, k).wait_recv())
+    for s in range(pairs):
         final = final + branch_in[s].astype(F32)
     fin_own[...] = final
-    fin_copy = pltpu.make_async_remote_copy(
-        src_ref=fin_own,
-        dst_ref=fin_pair,
-        send_sem=pair_sem.at[2],
-        recv_sem=pair_sem.at[3],
-        device_id={"ep": partner},
-        device_id_type=MESH,
-    )
+    fin_copy = pair_copy(1, fin_own, fin_pair)
     fin_copy.start()
-    ones = jnp.ones((stat_own.shape[0], block), F32)
+    ones = jnp.ones((8, block), F32)
     sums = dot_nt(ones, final, HIGH)
     squares = dot_nt(ones, final * final, HIGH)
     stat_own[...] = jnp.zeros_like(stat_own)
-    stat_own[:, 0:half] = jnp.where(iota(sums.shape, 0) == 0, sums, squares)
+    stat_own[:, 0:half] = sums[0:1, :]
+    stat_own[:, half : 2 * half] = squares[0:1, :]
 
     def copy_stat(d, origin):
         return remote(7, stat_own, stat_in.at[origin], d, d, origin)
@@ -395,23 +443,22 @@
         stat = stat_in[p]
         for s in range(p + 2, devices, 2):
             stat = stat + stat_in[s]
-        center = column_of(stat[0:1, :], half) / model
-        second = column_of(stat[1:2, :], half) / model
+        center = column_of(stat, half) / model
+        second = column_of(stat, half, half) / model
         value = jnp.where(side == p, final, other_final)
         unit = (value - center) * lax.rsqrt(second - center * center + norm_eps)
         unit = jnp.where(side == 0, unit, pltpu.roll(unit, feat, 1))
         out[p * half : (p + 1) * half, :] = (unit[:, 0:feat] * gain).astype(BF16)
 
-    each(devices, me, lambda d: copy_proj(d, me).wait_send())
-    each(devices, me, lambda d: copy_forget(d, me).wait_send())
-    each(devices, me, lambda d: copy_wout(d, me).wait_send())
+    each(groups_f, group_f, lambda g: copy_forget(g, group_f).wait_send())
+    each(per_f, member_f, lambda m: copy_quad(m, member_f).wait_send())
     each(members, member, lambda m: copy_group(m, member).wait_send())
     each(devices, me, lambda d: copy_attn(d, me).wait_send())
-    each(pairs, pair, lambda k: copy_mixed(k, pair).wait_send())
-    each(devices, me, lambda d: copy_branch(d, me).wait_send())
     each(devices, me, lambda d: copy_stat(d, me).wait_send())
-    tok_copy.wait_send()
-    fin_copy.wait_send()
+    for copy in (copy_proj, copy_wout, copy_mixed, copy_branch):
+        each(pairs, pair, lambda k: copy(k, pair).wait_send())
+    for copy in (proj_copy, tok_copy, wout_copy, branch_copy, fin_copy):
+        copy.wait_send()
 
 
 def shards(
@@ -448,12 +495,14 @@
     block = 2 * feat
     half = seqs // 2
     pieces = width // LANES
+    pairs = devices // 2
+    per_f = rows_f // seqs_here
     vmem = pl.BlockSpec(memory_space=pltpu.VMEM)
     hbm = pl.BlockSpec(memory_space=pl.ANY)
     big = (
         cache_keys,
         cache_values,
-        cache_gates,
+        jnp.transpose(cache_gates, (0, 2, 1)),
         expert_w_gate,
         expert_w_up,
         dense_w_gate,
@@ -469,14 +518,17 @@
         scratch_shapes=[pltpu.VMEM(a.shape, a.dtype) for a in big]
         + [
             pltpu.VMEM((seqs, 3 * width), BF16),
-            pltpu.VMEM((devices, rows_p, cols_p), BF16),
+            pltpu.VMEM((seqs, 3 * width // 2), BF16),
+            pltpu.VMEM((seqs, 3 * width // 2), BF16),
+            pltpu.VMEM((pairs, rows_p, cols_p), BF16),
             pltpu.VMEM((rows_p, cols_p), BF16),
             pltpu.VMEM((rows_p, 3 * width), BF16),
             pltpu.VMEM((seqs, LANES), F32),
-            pltpu.VMEM((devices, rows_f, LANES), F32),
+            pltpu.VMEM((seqs // rows_f, rows_f, LANES), F32),
+            pltpu.VMEM((per_f, rows_f, LANES), F32),
             pltpu.VMEM((seqs, block), BF16),
             pltpu.VMEM((seqs, block), BF16),
-            pltpu.VMEM((devices, width // devices, block), BF16),
+            pltpu.VMEM((pairs, 2, width // devices, block), BF16),
             pltpu.VMEM((seqs_here * pieces, LANES), F32),
             pltpu.VMEM((seqs_here * pieces, LANES), BF16),
             pltpu.VMEM((devices, seqs_here * pieces, LANES), BF16),
@@ -484,15 +536,17 @@
             pltpu.VMEM((seqs, model), BF16),
             pltpu.VMEM((seqs, model), BF16),
             pltpu.VMEM((seqs, model), BF16),
-            pltpu.VMEM((devices, half, block), BF16),
+            pltpu.VMEM((half, model), BF16),
+            pltpu.VMEM((half, model), BF16),
+            pltpu.VMEM((pairs, half, block), BF16),
             pltpu.VMEM((half, block), F32),
             pltpu.VMEM((half, block), F32),
-            pltpu.VMEM((8, LANES), F32),
-            pltpu.VMEM((devices, 8, LANES), F32),
+            pltpu.VMEM((1, LANES), F32),
+            pltpu.VMEM((devices, 1, LANES), F32),
             pltpu.SemaphoreType.DMA((len(big),)),
-            pltpu.SemaphoreType.DMA((8, devices)),
-            pltpu.SemaphoreType.DMA((8, devices)),
-            pltpu.SemaphoreType.DMA((4,)),
+            pltpu.SemaphoreType.DMA((9, devices)),
+            pltpu.SemaphoreType.DMA((9, devices)),
+            pltpu.SemaphoreType.DMA((10,)),
         ],
         compiler_params=pltpu.CompilerParams(
             collective_id=0, has_side_effects=True, vmem_limit_bytes=60 * 1024 * 1024
@@ -503,13 +557,13 @@
         w_query,
         w_key,
         w_value,
-        w_forget,
+        w_forget.T,
         forget_bias[None, :],
         w_out,
-        norm_gain[None, :],
-        w_router,
-        routes,
-        dense_gate[None, :],
+        norm_gain.reshape(-1, LANES),
+        w_router.T,
+        routes.T,
+        dense_gate.reshape(-1, LANES),
         final_gain[None, :],
         *big,
     )

time: 75.5 us -> 59.9 us (0.79)
  local copies, waits for them, and re-layouts: 10.7 us -> 1.32 us
  Pallas kernels: 64.4 us -> 58.3 us
    unnamed x5 -> x1, local copies, waits for them, and re-layouts: 8.09 us -> 1.32 us
    pallas_call x1, Pallas kernels: 64.4 us -> 58.3 us  [shards(): pl.pallas_call(functools.partial(layer_kernel, devices), out_shape=jax.Sh...]
    broadcast_in_dim x2 -> x0, local copies, waits for them, and re-layouts: 2.57 us -> none  [the longest x1 1.28 us: shards(): dense_gate[None, :]]
where the time goes in v2:
time: 59.9 us; the launch traced here: 59.6 us
  Pallas kernels  58.3 us (97%)
  local copies, waits for them, and re-layouts  1.32 us (2%)
    pallas_call x1, Pallas kernels, shards(): pl.pallas_call(functools.partial(layer_kernel, devices), out_shape=jax.Sh...  58.3 us
    unnamed x1, local copies, waits for them, and re-layouts  1.32 us

profile of v2, /device:TPU:0, one launch (start us, length us, event | category | flops | bytes accessed | tf_op | source)
XLA Modules:
  0.0 59.6 jit_solution(1720356055548137110)
XLA Ops:
  0.0 58.3 %shard_map.208 = bf16[64,64]{1,0:T(8,128)(2,1)} custom-call(s32[2]{0:T(128)} %lengths.1, bf16[64,64]{1,0:T(8,128)(2,1)} %tokens.1, bf16[64,1024]{1,0:T(8,128)(2,1)} %w_query.1, bf16[64,1024]{1,0:T(8,128)(2,1)} %w_key.1, bf16[64,1024]{1,0:T(8,128)(2,1)} %w_value.1, bf16[16,64]{1,0:T(8,128)(2,1)} %bitcast.10, f32[1,16]{1,0:T(1,128)} %bitcast.14, ...), custom_call_target="tpu_custom_call" | custom-call | tf_op jit(solution)/shard_map/pallas_call | solution.py:513
  58.3 1.3 %copy.24 = bf16[64,64]{1,0:T(8,128)(2,1)} copy(bf16[64,64]{1,0:T(8,128)(2,1)} %shard_map.208) | data formatting | bytes 16384

commit v3 on v2

--- a/solution.py
+++ b/solution.py
@@ -322,28 +322,63 @@
             attn_f[at : at + 1, :] = attn_row[:, j * LANES : (j + 1) * LANES]
     attn_own[...] = attn_f[...].astype(BF16)
 
-    def copy_attn(d, origin):
-        return remote(4, attn_own, attn_in.at[origin], d, d, origin)
-
-    each(devices, me, lambda d: copy_attn(d, me).start())
-    attn_in[me] = attn_own[...]
+    share_of = devices // 2
+    rank_half = me // share_of
+    rank_slot = me % share_of
+
+    def half_rows(at):
+        return pl.ds(pl.multiple_of(half * at, half), half)
+
+    def copy_attn(k, origin):
+        return remote(4, attn_own, attn_in.at[origin], 2 * k + rank_half, k, origin)
+
+    def attn_sends(fn):
+        def body(step, carry):
+            k = (pair + step) % pairs
+
+            @pl.when(2 * k + rank_half != me)
+            def _():
+                fn(copy_attn(k, rank_slot))
+
+            return carry
+
+        lax.fori_loop(0, pairs, body, 0)
+
+    def attn_arrivals():
+        def body(j, carry):
+            @pl.when(share_of * side + j != me)
+            def _():
+                copy_attn(j, j).wait_recv()
+
+            return carry
+
+        lax.fori_loop(0, share_of, body, 0)
+
+    attn_sends(lambda copy: copy.start())
+
+    @pl.when(rank_half == side)
+    def _():
+        attn_in[rank_slot] = attn_own[...]
+
     tok_copy.wait_recv()
-    residual = residual_scale * (tok_own[...].astype(F32) + tok_pair[...].astype(F32))
+    residual = residual_scale * (
+        tok_own[half_rows(side), :].astype(F32) + tok_pair[half_rows(side), :].astype(F32)
+    )
     each(pairs, pair, lambda k: copy_wout(k, k).wait_recv())
     wout_copy = pair_copy(3, wcol.at[:, side], wcol.at[:, side])
     wout_copy.start()
     wout_copy.wait_recv()
-    each(devices, me, lambda d: copy_attn(d, d).wait_recv())
+    attn_arrivals()
 
     pieces = width // LANES
-    attn_all = attn_in[...].reshape(seqs * pieces, LANES)
+    attn_all = attn_in[...].reshape(half * pieces, LANES)
     w_cols = wcol[...].reshape(width, block)
-    acc = jnp.zeros((seqs * pieces, block), F32)
-    turn = iota((seqs * pieces, block), 0) % pieces
+    acc = jnp.zeros((half * pieces, block), F32)
+    turn = iota((half * pieces, block), 0) % pieces
     for j in range(pieces):
         part = dot(attn_all, w_cols[j * LANES : (j + 1) * LANES, :])
         acc = jnp.where(turn == j, part, acc)
-    mixed = residual + jnp.sum(acc.reshape(seqs, pieces, block), axis=1)
+    mixed = residual + jnp.sum(acc.reshape(half, pieces, block), axis=1)
     mixed_own[...] = mixed.astype(BF16)
 
     def copy_mixed(k, origin):
@@ -368,7 +403,13 @@
         * lax.rsqrt(second - center * center + norm_eps)
         * row_of(norm_gain[...])
     ).astype(BF16)
-    normed_v[...] = normed
+    normed_v[half_rows(side), :] = normed
+    normed_copy = pair_copy(
+        5, normed_v.at[half_rows(side)], normed_v.at[half_rows(side)]
+    )
+    normed_copy.start()
+    normed_copy.wait_recv()
+    normed = normed_v[...]
 
     logits = dot_nt(normed, w_router[...])
     names = routes[...].astype(F32)
@@ -398,9 +439,6 @@
     loads[8].wait()
     branch_v[...] = (dot(hidden_e, ed_v[...]) + dot(hidden_d, dd_v[...])).astype(BF16)
 
-    def half_rows(at):
-        return pl.ds(pl.multiple_of(half * at, half), half)
-
     branch_copy = pair_copy(4, branch_v.at[half_rows(1 - side)], branch_pair)
     branch_copy.start()
     final = residual_scale * normed_v[half_rows(side), block_cols(pair)].astype(F32)
@@ -453,11 +491,11 @@
     each(groups_f, group_f, lambda g: copy_forget(g, group_f).wait_send())
     each(per_f, member_f, lambda m: copy_quad(m, member_f).wait_send())
     each(members, member, lambda m: copy_group(m, member).wait_send())
-    each(devices, me, lambda d: copy_attn(d, me).wait_send())
+    attn_sends(lambda copy: copy.wait_send())
     each(devices, me, lambda d: copy_stat(d, me).wait_send())
     for copy in (copy_proj, copy_wout, copy_mixed, copy_branch):
         each(pairs, pair, lambda k: copy(k, pair).wait_send())
-    for copy in (proj_copy, tok_copy, wout_copy, branch_copy, fin_copy):
+    for copy in (proj_copy, tok_copy, wout_copy, normed_copy, branch_copy, fin_copy):
         copy.wait_send()
 
 
@@ -531,9 +569,9 @@
             pltpu.VMEM((pairs, 2, width // devices, block), BF16),
             pltpu.VMEM((seqs_here * pieces, LANES), F32),
             pltpu.VMEM((seqs_here * pieces, LANES), BF16),
-            pltpu.VMEM((devices, seqs_here * pieces, LANES), BF16),
-            pltpu.VMEM((seqs, block), BF16),
-            pltpu.VMEM((seqs, model), BF16),
+            pltpu.VMEM((pairs, seqs_here * pieces, LANES), BF16),
+            pltpu.VMEM((half, block), BF16),
+            pltpu.VMEM((half, model), BF16),
             pltpu.VMEM((seqs, model), BF16),
             pltpu.VMEM((seqs, model), BF16),
             pltpu.VMEM((half, model), BF16),
@@ -546,7 +584,7 @@
             pltpu.SemaphoreType.DMA((len(big),)),
             pltpu.SemaphoreType.DMA((9, devices)),
             pltpu.SemaphoreType.DMA((9, devices)),
-            pltpu.SemaphoreType.DMA((10,)),
+            pltpu.SemaphoreType.DMA((12,)),
         ],
         compiler_params=pltpu.CompilerParams(
             collective_id=0, has_side_effects=True, vmem_limit_bytes=60 * 1024 * 1024

time: 59.9 us -> 56.7 us (0.947)
  Pallas kernels: 58.3 us -> 55.1 us
    pallas_call x1, Pallas kernels: 58.3 us -> 55.1 us  [shards(): pl.pallas_call(functools.partial(layer_kernel, devices), out_shape=jax.Sh...]
where the time goes in v3:
time: 56.7 us; the launch traced here: 56.5 us
  Pallas kernels  55.1 us (97%)
  local copies, waits for them, and re-layouts  1.32 us (2%)
    pallas_call x1, Pallas kernels, shards(): pl.pallas_call(functools.partial(layer_kernel, devices), out_shape=jax.Sh...  55.1 us
    unnamed x1, local copies, waits for them, and re-layouts  1.32 us

profile of v3, /device:TPU:0, one launch (start us, length us, event | category | flops | bytes accessed | tf_op | source)
XLA Modules:
  0.0 56.5 jit_solution(14042153212819381490)
XLA Ops:
  0.0 55.1 %shard_map.208 = bf16[64,64]{1,0:T(8,128)(2,1)} custom-call(s32[2]{0:T(128)} %lengths.1, bf16[64,64]{1,0:T(8,128)(2,1)} %tokens.1, bf16[64,1024]{1,0:T(8,128)(2,1)} %w_query.1, bf16[64,1024]{1,0:T(8,128)(2,1)} %w_key.1, bf16[64,1024]{1,0:T(8,128)(2,1)} %w_value.1, bf16[16,64]{1,0:T(8,128)(2,1)} %bitcast.10, f32[1,16]{1,0:T(1,128)} %bitcast.14, ...), custom_call_target="tpu_custom_call" | custom-call | tf_op jit(solution)/shard_map/pallas_call | solution.py:551
  55.1 1.3 %copy.24 = bf16[64,64]{1,0:T(8,128)(2,1)} copy(bf16[64,64]{1,0:T(8,128)(2,1)} %shard_map.208) | data formatting | bytes 16384
